TPU v7x, 32 devices: a whole 2x2x4 slice. The times are simulated.
32 devices in a mesh: ep: 8 (over z, core), tp: 4 (over y, x).
Axes of the slice: x: 2, y: 2, z: 4, core: 2. Of those that a mesh axis runs over, the one named last changes fastest.
Arguments:
- tokens: bfloat16 [256, 4096], P('ep'), may hold values from -6 to 6
- recur_state: float32 [256, 4096], P('ep', 'tp'), may hold values from -6 to 6
- conv_state: bfloat16 [256, 3, 4096], P('ep', None, 'tp'), may hold values from -6 to 6
- mix_gain: float32 [4096], replicated, may hold values from 0.1 to 1.9
- in_weight: bfloat16 [4096, 4096], P('ep', 'tp'), may hold values from -0.09375 to 0.09375
- gate_weight: bfloat16 [4096, 4096], P('ep', 'tp'), may hold values from -0.09375 to 0.09375
- conv_taps: float32 [4, 4096], P(None, 'tp'), may hold values from -3 to 3
- recur_gate_blocks: bfloat16 [64, 64, 64], P('tp'), may hold values from -0.75 to 0.75
- input_gate_blocks: bfloat16 [64, 64, 64], P('tp'), may hold values from -0.75 to 0.75
- decay_rate: float32 [4096], P('tp'), may hold values from 0.01 to 0.4
- out_weight: bfloat16 [4096, 4096], P('tp', 'ep'), may hold values from -0.09375 to 0.09375
- ffn_gain: float32 [4096], replicated, may hold values from 0.1 to 1.9
- router_weight: bfloat16 [4096, 8], replicated, may hold values from -0.09375 to 0.09375
- routes: int32 [256, 2], P('ep'), may hold values from 0 to 7, as said below
- expert_gate: bfloat16 [8, 4096, 2048], P('ep', None, 'tp'), may hold values from -0.09375 to 0.09375
- expert_up: bfloat16 [8, 4096, 2048], P('ep', None, 'tp'), may hold values from -0.09375 to 0.09375
- expert_down: bfloat16 [8, 2048, 4096], P('ep', 'tp'), may hold values from -0.125 to 0.125
- dense_gate: bfloat16 [4096, 2048], P('ep', 'tp'), may hold values from -0.09375 to 0.09375
- dense_up: bfloat16 [4096, 2048], P('ep', 'tp'), may hold values from -0.09375 to 0.09375
- dense_down: bfloat16 [2048, 4096], P('tp', 'ep'), may hold values from -0.125 to 0.125
- branch_gate: bfloat16 [4096], replicated, may hold values from -0.09375 to 0.09375
Outputs:
- layer_out: bfloat16 [256, 4096], P('ep')
- new_state: float32 [256, 4096], P('ep', 'tp')
- new_conv_state: bfloat16 [256, 3, 4096], P('ep', None, 'tp')
Inputs may be any that keep to these rules, and one draw needn't show every extreme that they name: `routes`: A row names two different experts of one group: both have the same e // 4. In the rows of one index of ep no expert is named more than 16 times, and in every draw some expert is named exactly 16 times by the rows of every index of ep.
All inputs are finite; a program needn't handle non-finite values.
Results may differ from a plain program's by a relative error of at most 0.023.
Values may be sent and summed in bfloat16 or wider, within the bound.
A program may use at most 64 MiB of HBM per device.

v0:
```python
import jax
import jax.numpy as jnp
from jax import lax
from jax.sharding import PartitionSpec as P

TOP_K = 2
epsilon = 1e-06
decay_scale = 8.0


def rms_scale(rows, gain):
    values = rows.astype(jnp.float32)
    inverse = lax.rsqrt(jnp.mean(values * values, axis=-1, keepdims=True) + epsilon)
    return (values * inverse * gain).astype(jnp.bfloat16)


def on_device(
    tokens,
    recur_state,
    conv_state,
    mix_gain,
    in_weight,
    gate_weight,
    conv_taps,
    recur_gate_blocks,
    input_gate_blocks,
    decay_rate,
    out_weight,
    ffn_gain,
    router_weight,
    routes,
    expert_gate,
    expert_up,
    expert_down,
    dense_gate,
    dense_up,
    dense_down,
    branch_gate,
):
    batch_rows, width = tokens.shape
    channels = in_weight.shape[1]
    normed = rms_scale(tokens, mix_gain)
    arrived = lax.all_to_all(normed, "ep", split_axis=1, concat_axis=0, tiled=True)
    joined = jnp.concatenate([in_weight, gate_weight], axis=1)
    summed = lax.psum_scatter(
        jnp.dot(arrived, joined, preferred_element_type=jnp.float32).astype(jnp.bfloat16),
        "ep",
        scatter_dimension=0,
        tiled=True,
    ).astype(jnp.float32)
    x_sum, gate_sum = (summed[:, :channels], summed[:, channels:])
    x_branch = x_sum.astype(jnp.bfloat16)
    gate_branch = gate_sum.astype(jnp.bfloat16)
    window = jnp.concatenate([conv_state, x_branch[:, None, :]], axis=1)
    conv_out = jnp.sum(window.astype(jnp.float32) * conv_taps[None], axis=1).astype(jnp.bfloat16)
    new_conv_state = window[:, 1:, :]
    blocks = conv_out.reshape(batch_rows, recur_gate_blocks.shape[0], recur_gate_blocks.shape[1])
    recur_gate = jax.nn.sigmoid(
        jnp.einsum(
            "bhi,hij->bhj", blocks, recur_gate_blocks, preferred_element_type=jnp.float32
        ).reshape(batch_rows, channels)
    )
    input_gate = jax.nn.sigmoid(
        jnp.einsum(
            "bhi,hij->bhj", blocks, input_gate_blocks, preferred_element_type=jnp.float32
        ).reshape(batch_rows, channels)
    )
    log_decay = -decay_scale * recur_gate * decay_rate
    new_state = jnp.exp(log_decay) * recur_state + jnp.sqrt(
        -jnp.expm1(2.0 * log_decay)
    ) * input_gate * conv_out.astype(jnp.float32)
    mixer_rows = (new_state * jax.nn.gelu(gate_branch.astype(jnp.float32))).astype(jnp.bfloat16)
    mixer_part = jnp.dot(
        mixer_rows,
        lax.all_gather(out_weight, "ep", axis=1, tiled=True),
        preferred_element_type=jnp.float32,
    )
    resid = (
        tokens.astype(jnp.float32)
        + lax.psum(mixer_part.astype(jnp.bfloat16), "tp").astype(jnp.float32)
    ).astype(jnp.bfloat16)
    normed_ffn = rms_scale(resid, ffn_gain)
    router_logits = jnp.dot(normed_ffn, router_weight, preferred_element_type=jnp.float32)
    experts = router_logits.shape[1]
    expert_ids = lax.broadcasted_iota(jnp.int32, (batch_rows, TOP_K, experts), 2)
    picked = jnp.sum(
        jnp.where(routes[:, :, None] == expert_ids, router_logits[:, None, :], 0.0), axis=2
    )
    route_weight = jax.nn.sigmoid(picked - picked[:, ::-1]).astype(jnp.bfloat16)
    capacity = 2 * batch_rows * TOP_K // experts
    flat_ids = routes.reshape(batch_rows * TOP_K)
    onehot = (
        flat_ids[:, None] == lax.broadcasted_iota(jnp.int32, (batch_rows * TOP_K, experts), 1)
    ).astype(jnp.int32)
    rank = jnp.sum((jnp.cumsum(onehot, axis=0) - onehot) * onehot, axis=1)
    slot_of = (flat_ids * capacity + rank).reshape(batch_rows, TOP_K)
    slot_rows = lax.broadcasted_iota(jnp.int32, (experts * capacity, batch_rows), 0)
    slot_cols = lax.broadcasted_iota(jnp.int32, (batch_rows, experts * capacity), 1)
    dispatch = jnp.zeros((experts * capacity, batch_rows), jnp.bfloat16)
    combine = jnp.zeros((batch_rows, experts * capacity), jnp.bfloat16)
    for pick in range(TOP_K):
        dispatch = dispatch + (slot_rows == slot_of[None, :, pick]).astype(jnp.bfloat16)
        combine = combine + jnp.where(
            slot_cols == slot_of[:, pick : pick + 1],
            route_weight[:, pick : pick + 1],
            jnp.zeros((), jnp.bfloat16),
        )
    outgoing = (
        jnp.dot(dispatch, normed_ffn, preferred_element_type=jnp.float32)
        .astype(jnp.bfloat16)
        .reshape(experts, capacity, width)
    )
    gate_local = expert_gate[0]
    up_local = expert_up[0]
    down_local = expert_down[0]
    arrived_rows = lax.all_to_all(outgoing, "ep", split_axis=0, concat_axis=0, tiled=True)
    sources, items, features = arrived_rows.shape
    rows = arrived_rows.reshape(sources * items, features)
    first = jnp.dot(rows, gate_local, preferred_element_type=jnp.float32)
    second = jnp.dot(rows, up_local, preferred_element_type=jnp.float32)
    act = (jax.nn.silu(first) * second).astype(jnp.bfloat16)
    partial_value = jnp.dot(act, down_local, preferred_element_type=jnp.float32)
    total = lax.psum(partial_value.astype(jnp.bfloat16), "tp")
    returned = lax.all_to_all(
        total.reshape(sources, items, total.shape[1]), "ep", split_axis=0, concat_axis=0, tiled=True
    )
    moe = jnp.dot(
        combine,
        returned.reshape(experts * capacity, returned.shape[2]),
        preferred_element_type=jnp.float32,
    )
    dense_arrived = lax.all_to_all(normed_ffn, "ep", split_axis=1, concat_axis=0, tiled=True)
    dense_joined = jnp.concatenate([dense_gate, dense_up], axis=1)
    dense_summed = lax.psum_scatter(
        jnp.dot(dense_arrived, dense_joined, preferred_element_type=jnp.float32).astype(
            jnp.bfloat16
        ),
        "ep",
        scatter_dimension=0,
        tiled=True,
    ).astype(jnp.float32)
    dense_first = dense_summed[:, : dense_gate.shape[1]]
    dense_second = dense_summed[:, dense_gate.shape[1] :]
    dense_act = (jax.nn.silu(dense_first) * dense_second).astype(jnp.bfloat16)
    dense_part = jnp.dot(
        dense_act,
        lax.all_gather(dense_down, "ep", axis=1, tiled=True),
        preferred_element_type=jnp.float32,
    )
    branch_weight = jax.nn.sigmoid(
        jnp.dot(normed_ffn, branch_gate, preferred_element_type=jnp.float32)
    )
    dense_sum = lax.psum(dense_part.astype(jnp.bfloat16), "tp").astype(jnp.float32)
    layer_out = (resid.astype(jnp.float32) + moe + branch_weight[:, None] * dense_sum).astype(
        jnp.bfloat16
    )
    return (layer_out, new_state, new_conv_state)


def solution(mesh):
    in_specs = (
        P("ep", None),
        P("ep", "tp"),
        P("ep", None, "tp"),
        P(),
        P("ep", "tp"),
        P("ep", "tp"),
        P(None, "tp"),
        P("tp", None, None),
        P("tp", None, None),
        P("tp"),
        P("tp", "ep"),
        P(),
        P(),
        P("ep", None),
        P("ep", None, "tp"),
        P("ep", None, "tp"),
        P("ep", "tp", None),
        P("ep", "tp"),
        P("ep", "tp"),
        P("tp", "ep"),
        P(),
    )
    out_specs = (P("ep", None), P("ep", "tp"), P("ep", None, "tp"))
    return jax.shard_map(
        on_device, mesh=mesh, in_specs=in_specs, out_specs=out_specs, check_vma=False
    )
```

profile of v0, /device:TPU:0, one launch (start us, length us, event | category | flops | bytes accessed | tf_op | source)
XLA Modules:
  0.0 396.9 jit_solution(11186199223250125864)
XLA Ops:
  7.2 1.1 fusion.33
  8.4 1.1 fusion.35
  9.5 16.0 %all_to_all.48 = bf16[32,8,512]{2,0,1:T(8,128)(2,1)S(1)} all-to-all(bf16[32,8,512]{2,0,1:T(8,128)(2,1)S(1)} %bitcast.77), channel_id=1, replica_groups=mesh['ep'=8,'tp'=4] {'ep'}, dimensions={1} | all-to-all | bytes 524288 | tf_op jit(solution)/shard_map/all_to_all | solution.py:43
  25.5 3.4 convolution_convert_fusion.4
  29.0 0.7 all-gather.3.cloned.1.call-update
  29.8 30.9 %reduce-scatter.3.cloned.1.call-done = bf16[32,2048]{1,0:T(8,128)(2,1)} async-done(((bf16[256,2048]{1,0:T(8,128)(2,1)}), bf16[32,2048]{1,0:T(8,128)(2,1)}) %reduce-scatter.3.cloned.1.call-update) | async-done | bytes 131088 | tf_op jit(solution)/shard_map/reduce_scatter | solution.py:45
  60.7 0.9 slice_bitcast_fusion
  61.9 0.2 fusion.17
  62.4 0.2 fusion.13
  63.1 79.5 %all-gather.3.cloned.1.call-done = bf16[1024,4096]{1,0:T(8,128)(2,1)} async-done(((bf16[1024,512]{1,0:T(8,128)(2,1)}), bf16[1024,4096]{1,0:T(8,128)(2,1)}) %all-gather.3.cloned.1.call-update) | async-done | bytes 8388624 | tf_op jit(solution)/shard_map/all_gather | solution.py:75
  142.5 5.6 %convolution_convert_fusion.3 = bf16[32,4096]{1,0:T(8,128)(2,1)} fusion(bf16[1024,4096]{1,0:T(8,128)(2,1)} %all-gather.3.cloned.1.call-done, f32[32,1024]{1,0:T(8,128)S(1)} %multiply_add_fusion, bf16[32,2048]{1,0:T(8,128)(2,1)S(1)} %copy-done.5), kind=kOutput, calls=%fused_computation.6 | convolution fusion | flops 268926976 | bytes 8847360 | tf_op jit(solution)/shard_map/dot_general | solution.py:73
  148.2 41.6 %all-reduce.4.cloned.1.call-done = bf16[32,4096]{1,0:T(8,128)(2,1)} async-done(((bf16[32,4096]{1,0:T(8,128)(2,1)}), bf16[32,4096]{1,0:T(8,128)(2,1)}) %all-reduce.4.cloned.1.call-update) | async-done | bytes 262160 | tf_op jit(solution)/shard_map/psum | solution.py:80
  189.9 1.1 fusion.37
  191.0 1.1 fusion.39
  192.1 14.1 %all_to_all.49 = bf16[32,8,512]{2,0,1:T(8,128)(2,1)S(1)} all-to-all(bf16[32,8,512]{2,0,1:T(8,128)(2,1)S(1)} %bitcast.78), channel_id=1, replica_groups=mesh['ep'=8,'tp'=4] {'ep'}, dimensions={1} | all-to-all | bytes 524288 | tf_op jit(solution)/shard_map/all_to_all | solution.py:132
  206.2 1.3 convolution_convert_fusion.5
  207.6 0.5 all-gather.5.cloned.1.call-update
  208.5 0.2 select_reduce_fusion
  208.9 1.4 convolution_convert_fusion.1
  210.3 3.6 all-to-all-start.1
  213.9 24.5 %reduce-scatter.5.cloned.1.call-done = bf16[32,1024]{1,0:T(8,128)(2,1)} async-done(((bf16[256,1024]{1,0:T(8,128)(2,1)}), bf16[32,1024]{1,0:T(8,128)(2,1)}) %reduce-scatter.5.cloned.1.call-update) | async-done | bytes 65552 | tf_op jit(solution)/shard_map/reduce_scatter | solution.py:134
  238.4 0.8 convert_element_type.109
  239.2 49.8 %all-gather.5.cloned.1.call-done = bf16[512,4096]{1,0:T(8,128)(2,1)} async-done(((bf16[512,512]{1,0:T(8,128)(2,1)}), bf16[512,4096]{1,0:T(8,128)(2,1)}) %all-gather.5.cloned.1.call-update) | async-done | bytes 4194320 | tf_op jit(solution)/shard_map/all_gather | solution.py:147
  289.0 3.7 convolution_convert_fusion.2
  292.7 2.9 fusion.5
  295.7 5.9 %convolution_convert_fusion = bf16[128,4096]{1,0:T(8,128)(2,1)} fusion(bf16[1,512,4096]{2,1,0:T(8,128)(2,1)} %param.37, bf16[128,4096]{1,0:T(8,128)(2,1)S(1)} %bitcast.72, bf16[1,4096,512]{2,1,0:T(8,128)(2,1)} %param.36, f32[128,512]{1,0:T(8,128)S(1)} %fusion.5), kind=kOutput, calls=%fused_computation | convolution fusion | flops 1074659328 | bytes 10747904 | tf_op jit(solution)/shard_map/dot_general | solution.py:122
  301.6 55.4 %all-reduce.6.cloned.1.call-done = (bf16[8,16,4096]{2,1,0:T(8,128)(2,1)}, bf16[32,4096]{1,0:T(8,128)(2,1)}) async-done(((bf16[8,16,4096]{2,1,0:T(8,128)(2,1)}, bf16[32,4096]{1,0:T(8,128)(2,1)}), (bf16[8,16,4096]{2,1,0:T(8,128)(2,1)}, bf16[32,4096]{1,0:T(8,128)(2,1)})) %all-reduce.6.cloned.1.call-update) | async-done | bytes 1310736 | tf_op jit(solution)/shard_map/psum | solution.py:123
  356.9 4.6 %all-to-all-start.2 = ((bf16[8,16,4096]{2,1,0:T(8,128)(2,1)}), bf16[8,16,4096]{2,1,0:T(8,128)(2,1)S(1)}, u32[]{:S(2)}, u32[]{:S(2)}) async-start(bf16[8,16,4096]{2,1,0:T(8,128)(2,1)} %get-tuple-element.3), calls=%async_computation.3 | async-start | bytes 2097152 | tf_op jit(solution)/shard_map/all_to_all | solution.py:124
  361.5 0.7 fusion.45
  362.5 0.2 fusion.27
  362.7 25.4 %all-to-all-done.2 = bf16[8,16,4096]{2,1,0:T(8,128)(2,1)S(1)} async-done(((bf16[8,16,4096]{2,1,0:T(8,128)(2,1)}), bf16[8,16,4096]{2,1,0:T(8,128)(2,1)S(1)}, u32[]{:S(2)}, u32[]{:S(2)}) %all-to-all-start.2) | async-done | bytes 1048608 | tf_op jit(solution)/shard_map/all_to_all | solution.py:124
  388.1 2.0 fusion.1
  (69 shorter events, 2.2 us)
Async XLA Ops:
  7.2 54.7 %copy-start = (bf16[16,64,64]{2,1,0:T(8,128)(2,1)S(1)}, bf16[16,64,64]{2,1,0:T(8,128)(2,1)}, u32[]{:S(2)}) copy-start(bf16[16,64,64]{2,1,0:T(8,128)(2,1)} %param.28) | copy-start | bytes 393220
  7.2 53.5 %reduce-scatter.3.cloned.1.call-start = ((), (), s32[]{:S(2)}) async-start(), calls=%async_computation.6 | async-start | bytes 1179648 | tf_op jit(solution)/shard_map/reduce_scatter | solution.py:45
  8.4 21.4 %copy-start.12 = (f32[1024]{0:T(1024)S(1)}, f32[1024]{0:T(1024)}, u32[]{:S(2)}) copy-start(f32[1024]{0:T(1024)} %param.30) | copy-start | bytes 12292
  9.5 52.1 %copy-start.4 = (bf16[32,3,1024]{2,0,1:T(8,128)(2,1)S(1)}, bf16[32,3,1024]{2,0,1:T(8,128)(2,1)}, u32[]{:S(2)}) copy-start(bf16[32,3,1024]{2,0,1:T(8,128)(2,1)} %param.23) | copy-start | bytes 589828
  9.5 52.1 %copy-start.9 = (f32[4,1024]{1,0:T(4,128)S(1)}, f32[4,1024]{1,0:T(4,128)}, u32[]{:S(2)}) copy-start(f32[4,1024]{1,0:T(4,128)} %param.27) | copy-start | bytes 49156
  25.5 36.8 %copy-start.15 = (bf16[16,64,64]{2,1,0:T(8,128)(2,1)S(1)}, bf16[16,64,64]{2,1,0:T(8,128)(2,1)}, u32[]{:S(2)}) copy-start(bf16[16,64,64]{2,1,0:T(8,128)(2,1)} %param.29) | copy-start | bytes 393220
  28.9 34.0 %copy-start.6 = (f32[32,1024]{1,0:T(8,128)S(1)}, f32[32,1024]{1,0:T(8,128)}, u32[]{:S(2)}) copy-start(f32[32,1024]{1,0:T(8,128)} %param.22) | copy-start | bytes 393220
  28.9 113.6 %all-gather.3.cloned.1.call-start = ((), (), s32[]{:S(2)}) async-start(), calls=%async_computation.7 | async-start | bytes 9437184 | tf_op jit(solution)/shard_map/all_gather | solution.py:75
  29.7 160.2 %all-reduce.4.cloned.1.call-start = ((), (), s32[]{:S(2)}) async-start(), calls=%async_computation.8 | async-start | bytes 524288 | tf_op jit(solution)/shard_map/psum | solution.py:80
  60.7 81.8 %copy-start.5 = (bf16[32,2048]{1,0:T(8,128)(2,1)S(1)}, bf16[32,2048]{1,0:T(8,128)(2,1)}, u32[]{:S(2)}) copy-start(bf16[32,2048]{1,0:T(8,128)(2,1)} %reduce-scatter.3.cloned.1.call-done) | copy-start | bytes 393220
  63.0 85.1 %copy-start.3 = (f32[32,1024]{1,0:T(8,128)}, f32[32,1024]{1,0:T(8,128)S(1)}, u32[]{:S(2)}) copy-start(f32[32,1024]{1,0:T(8,128)S(1)} %multiply_add_fusion) | copy-start | bytes 393220
  63.0 126.8 %copy-start.1 = (bf16[32,4096]{1,0:T(8,128)(2,1)S(1)}, bf16[32,4096]{1,0:T(8,128)(2,1)}, u32[]{:S(2)}) copy-start(bf16[32,4096]{1,0:T(8,128)(2,1)} %param.21) | copy-start | bytes 786436
  63.0 128.0 %copy-start.8 = (f32[4096]{0:T(1024)S(1)}, f32[4096]{0:T(1024)}, u32[]{:S(2)}) copy-start(f32[4096]{0:T(1024)} %param.32) | copy-start | bytes 49156
  63.1 143.2 %copy-start.13 = (bf16[512,512]{1,0:T(8,128)(2,1)S(1)}, bf16[512,512]{1,0:T(8,128)(2,1)}, u32[]{:S(2)}) copy-start(bf16[512,512]{1,0:T(8,128)(2,1)} %param.39) | copy-start | bytes 1572868
  63.1 143.2 %copy-start.14 = (bf16[512,512]{1,0:T(8,128)(2,1)S(1)}, bf16[512,512]{1,0:T(8,128)(2,1)}, u32[]{:S(2)}) copy-start(bf16[512,512]{1,0:T(8,128)(2,1)} %param.38) | copy-start | bytes 1572868
  148.2 60.0 %copy-start.10 = (s32[32,2]{0,1:T(2,128)S(1)}, s32[32,2]{0,1:T(2,128)}, u32[]{:S(2)}) copy-start(s32[32,2]{0,1:T(2,128)} %param.34) | copy-start | bytes 772
  148.2 90.2 %reduce-scatter.5.cloned.1.call-start = ((), (), s32[]{:S(2)}) async-start(), calls=%async_computation.9 | async-start | bytes 589824 | tf_op jit(solution)/shard_map/reduce_scatter | solution.py:134
  207.6 81.4 %all-gather.5.cloned.1.call-start = ((), (), s32[]{:S(2)}) async-start(), calls=%async_computation.10 | async-start | bytes 4718592 | tf_op jit(solution)/shard_map/all_gather | solution.py:147
  210.3 82.4 %all-to-all-start.1 = ((bf16[8,16,4096]{2,1,0:T(8,128)(2,1)}), bf16[8,16,4096]{2,1,0:T(8,128)(2,1)S(1)}, u32[]{:S(2)}, u32[]{:S(2)}) async-start(bf16[8,16,4096]{2,1,0:T(8,128)(2,1)} %bitcast.9), calls=%async_computation.2 | async-start | bytes 2097152 | tf_op jit(solution)/shard_map/all_to_all | solution.py:116
  213.9 143.0 %all-reduce.6.cloned.1.call-start = ((), (), s32[]{:S(2)}) async-start(), calls=%async_computation.11 | async-start | bytes 2621440 | tf_op jit(solution)/shard_map/psum | solution.py:123
  295.6 65.9 %copy-start.11 = (bf16[4096]{0:T(1024)(128)(2,1)S(1)}, bf16[4096]{0:T(1024)(128)(2,1)}, u32[]{:S(2)}) copy-start(bf16[4096]{0:T(1024)(128)(2,1)} %param.41) | copy-start | bytes 24580
  295.6 66.6 %copy-start.7 = (bf16[4096,8]{0,1:T(8,128)(2,1)S(1)}, bf16[4096,8]{0,1:T(8,128)(2,1)}, u32[]{:S(2)}) copy-start(bf16[4096,8]{0,1:T(8,128)(2,1)} %param.33) | copy-start | bytes 196612
  301.5 86.5 %copy-start.2 = (bf16[32,4096]{1,0:T(8,128)(2,1)S(1)}, bf16[32,4096]{1,0:T(8,128)(2,1)}, u32[]{:S(2)}) copy-start(bf16[32,4096]{1,0:T(8,128)(2,1)} %all-reduce.4.cloned.1.call-done) | copy-start | bytes 786436
  356.9 31.2 %all-to-all-start.2 = ((bf16[8,16,4096]{2,1,0:T(8,128)(2,1)}), bf16[8,16,4096]{2,1,0:T(8,128)(2,1)S(1)}, u32[]{:S(2)}, u32[]{:S(2)}) async-start(bf16[8,16,4096]{2,1,0:T(8,128)(2,1)} %get-tuple-element.3), calls=%async_computation.3 | async-start | bytes 2097152 | tf_op jit(solution)/shard_map/all_to_all | solution.py:124
Sparse Core Ops, SparseCore 0:
  29.1 31.6 reduce-scatter.2
  62.3 80.1 all-gather.2
  148.3 41.5 all-reduce.3
  207.7 30.6 reduce-scatter.4
  239.8 49.1 all-gather.4
  301.7 55.1 all-reduce.5
where the time goes:
time: 398 us; the launch traced here: 397 us
  waiting for transfers between devices  308 us (77%)
  blocking collectives  30.1 us (8%)
  matrix products  26.9 us (7%)
  between operations  14.4 us (4%)
  starting transfers between devices  8.4 us (2%)
  other arithmetic  6.59 us (2%)
    all_gather x1, waiting for transfers between devices, on_device(): lax.all_gather(out_weight, 'ep', axis=1, tiled=True)  79.5 us
    psum x1, waiting for transfers between devices, on_device(): total = lax.psum(partial_value.astype(jnp.bfloat16), 'tp')  55.4 us
    all_gather x1, waiting for transfers between devices, on_device(): lax.all_gather(dense_down, 'ep', axis=1, tiled=True)  49.8 us
    psum x1, waiting for transfers between devices, on_device(): lax.psum(mixer_part.astype(jnp.bfloat16), 'tp').astype(jnp.float32)  41.6 us
    reduce_scatter x1, waiting for transfers between devices, on_device(): lax.psum_scatter(jnp.dot(arrived, joined, preferred_element_type=jnp.floa...  30.9 us
    all_to_all x1, waiting for transfers between devices, on_device(): lax.all_to_all(total.reshape(sources, items, total.shape[1]), 'ep', split...  25.4 us
    reduce_scatter x1, waiting for transfers between devices, on_device(): lax.psum_scatter(jnp.dot(dense_arrived, dense_joined, preferred_element_t...  24.5 us
    all_to_all x1, blocking collectives, on_device(): lax.all_to_all(normed, 'ep', split_axis=1, concat_axis=0, tiled=True)  16 us
  transfers between devices with their start and end apart: 8, of which 7 were waited for; matrix products, arithmetic and copies ran while one was open for 3% of the time, Pallas kernels for 0%

commit v1 on v0

--- a/solution.py
+++ b/solution.py
@@ -6,6 +6,11 @@
 TOP_K = 2
 epsilon = 1e-06
 decay_scale = 8.0
+
+
+def all_parts(value, axis, d):
+    blocks = lax.all_gather(value, axis)
+    return jnp.concatenate(blocks, axis=d)
 
 
 def rms_scale(rows, gain):
@@ -71,9 +76,7 @@
     ) * input_gate * conv_out.astype(jnp.float32)
     mixer_rows = (new_state * jax.nn.gelu(gate_branch.astype(jnp.float32))).astype(jnp.bfloat16)
     mixer_part = jnp.dot(
-        mixer_rows,
-        lax.all_gather(out_weight, "ep", axis=1, tiled=True),
-        preferred_element_type=jnp.float32,
+        mixer_rows, all_parts(out_weight, "ep", 1), preferred_element_type=jnp.float32
     )
     resid = (
         tokens.astype(jnp.float32)

time: 398 us -> 410 us (1.030)
  local copies, waits for them, and re-layouts: 2.18 us -> 13.6 us
    reshape x0 -> x1, local copies, waits for them, and re-layouts: none -> 11.5 us  [all_parts(): return jnp.concatenate(blocks, axis=d)]
  transfers between devices with their start and end apart: 8 -> 8, of which waited for: 7 -> 7; matrix products, arithmetic and copies ran while one was open for 3% -> 2% of each run, Pallas kernels for 0% -> 0%
where the time goes in v1:
time: 410 us
  waiting for transfers between devices  308 us (75%)
  blocking collectives  30.1 us (7%)
  matrix products  28 us (7%)
  between operations  14.4 us (4%)
  local copies, waits for them, and re-layouts  13.6 us (3%)
  starting transfers between devices  8.4 us (2%)
  other arithmetic  6.59 us (2%)
    all_gather x1, waiting for transfers between devices, all_parts(): blocks = lax.all_gather(value, axis)  79.6 us
    psum x1, waiting for transfers between devices, on_device(): total = lax.psum(partial_value.astype(jnp.bfloat16), 'tp')  55.3 us
    all_gather x1, waiting for transfers between devices, on_device(): lax.all_gather(dense_down, 'ep', axis=1, tiled=True)  49.8 us
    psum x1, waiting for transfers between devices, on_device(): lax.psum(mixer_part.astype(jnp.bfloat16), 'tp').astype(jnp.float32)  41.6 us
    reduce_scatter x1, waiting for transfers between devices, on_device(): lax.psum_scatter(jnp.dot(arrived, joined, preferred_element_type=jnp.floa...  30.9 us
    all_to_all x1, waiting for transfers between devices, on_device(): lax.all_to_all(total.reshape(sources, items, total.shape[1]), 'ep', split...  25.4 us
    reduce_scatter x1, waiting for transfers between devices, on_device(): lax.psum_scatter(jnp.dot(dense_arrived, dense_joined, preferred_element_t...  24.5 us
    all_to_all x1, blocking collectives, on_device(): lax.all_to_all(normed, 'ep', split_axis=1, concat_axis=0, tiled=True)  16 us
  transfers between devices with their start and end apart: 8, of which 7 were waited for; matrix products, arithmetic and copies ran while one was open for 2% of the time, Pallas kernels for 0%

profile of v1, /device:TPU:0, one launch (start us, length us, event | category | flops | bytes accessed | tf_op | source)
XLA Modules:
  0.0 409.5 jit_solution(11488665345489946718)
XLA Ops:
  7.2 1.1 fusion.33
  8.4 1.1 fusion.35
  9.5 16.0 %all_to_all.48 = bf16[32,8,512]{2,0,1:T(8,128)(2,1)S(1)} all-to-all(bf16[32,8,512]{2,0,1:T(8,128)(2,1)S(1)} %bitcast.83), channel_id=1, replica_groups=mesh['ep'=8,'tp'=4] {'ep'}, dimensions={1} | all-to-all | bytes 524288 | tf_op jit(solution)/shard_map/all_to_all | solution.py:48
  25.5 3.4 convolution_convert_fusion.4
  29.0 0.7 all-gather.6.cloned.1.call-update
  29.7 30.9 %reduce-scatter.3.cloned.1.call-done = bf16[32,2048]{1,0:T(8,128)(2,1)} async-done(((bf16[256,2048]{1,0:T(8,128)(2,1)}), bf16[32,2048]{1,0:T(8,128)(2,1)}) %reduce-scatter.3.cloned.1.call-update) | async-done | bytes 131088 | tf_op jit(solution)/shard_map/reduce_scatter | solution.py:50
  60.7 0.8 slice_bitcast_fusion
  61.8 0.2 fusion.13
  62.3 0.2 fusion.17
  62.9 79.6 %all-gather.6.cloned.1.call-done = bf16[8192,512]{1,0:T(8,128)(2,1)} async-done(((bf16[1024,512]{1,0:T(8,128)(2,1)}), bf16[8192,512]{1,0:T(8,128)(2,1)}) %all-gather.6.cloned.1.call-update) | async-done | bytes 8388624 | tf_op jit(solution)/shard_map/all_gather | solution.py:12
  142.5 11.5 %copy.71 = bf16[1024,8,512]{0,2,1:T(8,128)(2,1)} copy(bf16[1024,8,512]{2,0,1:T(8,128)(2,1)} %bitcast.78) | data formatting | bytes 16777216 | tf_op jit(solution)/shard_map/reshape | solution.py:13
  154.0 6.7 %convolution_convert_fusion.3 = bf16[32,4096]{1,0:T(8,128)(2,1)} fusion(bf16[1024,4096]{0,1:T(8,128)(2,1)} %bitcast.75, f32[32,1024]{1,0:T(8,128)S(1)} %multiply_add_fusion, bf16[32,2048]{1,0:T(8,128)(2,1)S(1)} %copy-done.5), kind=kOutput, calls=%fused_computation.6 | convolution fusion | flops 268926976 | bytes 8847360 | tf_op jit(solution)/shard_map/dot_general | solution.py:78
  160.8 41.6 %all-reduce.4.cloned.1.call-done = bf16[32,4096]{1,0:T(8,128)(2,1)} async-done(((bf16[32,4096]{1,0:T(8,128)(2,1)}), bf16[32,4096]{1,0:T(8,128)(2,1)}) %all-reduce.4.cloned.1.call-update) | async-done | bytes 262160 | tf_op jit(solution)/shard_map/psum | solution.py:83
  202.5 1.1 fusion.37
  203.6 1.1 fusion.39
  204.7 14.1 %all_to_all.49 = bf16[32,8,512]{2,0,1:T(8,128)(2,1)S(1)} all-to-all(bf16[32,8,512]{2,0,1:T(8,128)(2,1)S(1)} %bitcast.84), channel_id=1, replica_groups=mesh['ep'=8,'tp'=4] {'ep'}, dimensions={1} | all-to-all | bytes 524288 | tf_op jit(solution)/shard_map/all_to_all | solution.py:135
  218.8 1.3 convolution_convert_fusion.5
  220.2 0.5 all-gather.4.cloned.1.call-update
  221.5 1.4 convolution_convert_fusion.1
  222.9 3.6 all-to-all-start.1
  226.5 24.5 %reduce-scatter.5.cloned.1.call-done = bf16[32,1024]{1,0:T(8,128)(2,1)} async-done(((bf16[256,1024]{1,0:T(8,128)(2,1)}), bf16[32,1024]{1,0:T(8,128)(2,1)}) %reduce-scatter.5.cloned.1.call-update) | async-done | bytes 65552 | tf_op jit(solution)/shard_map/reduce_scatter | solution.py:137
  251.0 0.8 convert_element_type.109
  251.8 49.8 %all-gather.4.cloned.1.call-done = bf16[512,4096]{1,0:T(8,128)(2,1)} async-done(((bf16[512,512]{1,0:T(8,128)(2,1)}), bf16[512,4096]{1,0:T(8,128)(2,1)}) %all-gather.4.cloned.1.call-update) | async-done | bytes 4194320 | tf_op jit(solution)/shard_map/all_gather | solution.py:150
  301.6 3.7 convolution_convert_fusion.2
  305.3 2.9 fusion.5
  308.2 5.9 %convolution_convert_fusion = bf16[128,4096]{1,0:T(8,128)(2,1)} fusion(bf16[1,512,4096]{2,1,0:T(8,128)(2,1)} %param.37, bf16[128,4096]{1,0:T(8,128)(2,1)S(1)} %bitcast.77, bf16[1,4096,512]{2,1,0:T(8,128)(2,1)} %param.36, f32[128,512]{1,0:T(8,128)S(1)} %fusion.5), kind=kOutput, calls=%fused_computation | convolution fusion | flops 1074659328 | bytes 10747904 | tf_op jit(solution)/shard_map/dot_general | solution.py:125
  314.2 55.3 %all-reduce.6.cloned.1.call-done = (bf16[8,16,4096]{2,1,0:T(8,128)(2,1)}, bf16[32,4096]{1,0:T(8,128)(2,1)}) async-done(((bf16[8,16,4096]{2,1,0:T(8,128)(2,1)}, bf16[32,4096]{1,0:T(8,128)(2,1)}), (bf16[8,16,4096]{2,1,0:T(8,128)(2,1)}, bf16[32,4096]{1,0:T(8,128)(2,1)})) %all-reduce.6.cloned.1.call-update) | async-done | bytes 1310736 | tf_op jit(solution)/shard_map/psum | solution.py:126
  369.5 4.6 %all-to-all-start.2 = ((bf16[8,16,4096]{2,1,0:T(8,128)(2,1)}), bf16[8,16,4096]{2,1,0:T(8,128)(2,1)S(1)}, u32[]{:S(2)}, u32[]{:S(2)}) async-start(bf16[8,16,4096]{2,1,0:T(8,128)(2,1)} %get-tuple-element.3), calls=%async_computation.3 | async-start | bytes 2097152 | tf_op jit(solution)/shard_map/all_to_all | solution.py:127
  374.1 0.7 fusion.45
  375.1 0.2 fusion.27
  375.3 25.4 %all-to-all-done.2 = bf16[8,16,4096]{2,1,0:T(8,128)(2,1)S(1)} async-done(((bf16[8,16,4096]{2,1,0:T(8,128)(2,1)}), bf16[8,16,4096]{2,1,0:T(8,128)(2,1)S(1)}, u32[]{:S(2)}, u32[]{:S(2)}) %all-to-all-start.2) | async-done | bytes 1048608 | tf_op jit(solution)/shard_map/all_to_all | solution.py:127
  400.7 2.0 fusion.1
  (70 shorter events, 2.3 us)
Async XLA Ops:
  7.2 54.6 %copy-start = (bf16[16,64,64]{2,1,0:T(8,128)(2,1)S(1)}, bf16[16,64,64]{2,1,0:T(8,128)(2,1)}, u32[]{:S(2)}) copy-start(bf16[16,64,64]{2,1,0:T(8,128)(2,1)} %param.29) | copy-start | bytes 393220
  7.2 53.5 %reduce-scatter.3.cloned.1.call-start = ((), (), s32[]{:S(2)}) async-start(), calls=%async_computation.6 | async-start | bytes 1179648 | tf_op jit(solution)/shard_map/reduce_scatter | solution.py:50
  8.4 21.3 %copy-start.12 = (f32[1024]{0:T(1024)S(1)}, f32[1024]{0:T(1024)}, u32[]{:S(2)}) copy-start(f32[1024]{0:T(1024)} %param.30) | copy-start | bytes 12292
  9.5 52.0 %copy-start.3 = (bf16[32,3,1024]{2,0,1:T(8,128)(2,1)S(1)}, bf16[32,3,1024]{2,0,1:T(8,128)(2,1)}, u32[]{:S(2)}) copy-start(bf16[32,3,1024]{2,0,1:T(8,128)(2,1)} %param.23) | copy-start | bytes 589828
  9.5 52.0 %copy-start.9 = (f32[4,1024]{1,0:T(4,128)S(1)}, f32[4,1024]{1,0:T(4,128)}, u32[]{:S(2)}) copy-start(f32[4,1024]{1,0:T(4,128)} %param.27) | copy-start | bytes 49156
  25.5 36.7 %copy-start.15 = (bf16[16,64,64]{2,1,0:T(8,128)(2,1)S(1)}, bf16[16,64,64]{2,1,0:T(8,128)(2,1)}, u32[]{:S(2)}) copy-start(bf16[16,64,64]{2,1,0:T(8,128)(2,1)} %param.28) | copy-start | bytes 393220
  28.9 33.9 %copy-start.6 = (f32[32,1024]{1,0:T(8,128)S(1)}, f32[32,1024]{1,0:T(8,128)}, u32[]{:S(2)}) copy-start(f32[32,1024]{1,0:T(8,128)} %param.22) | copy-start | bytes 393220
  28.9 113.6 %all-gather.6.cloned.1.call-start = ((), (), s32[]{:S(2)}) async-start(), calls=%async_computation.10 | async-start | bytes 9437184 | tf_op jit(solution)/shard_map/all_gather | solution.py:12
  29.7 172.8 %all-reduce.4.cloned.1.call-start = ((), (), s32[]{:S(2)}) async-start(), calls=%async_computation.7 | async-start | bytes 524288 | tf_op jit(solution)/shard_map/psum | solution.py:83
  62.9 91.0 %copy-start.4 = (f32[32,1024]{1,0:T(8,128)}, f32[32,1024]{1,0:T(8,128)S(1)}, u32[]{:S(2)}) copy-start(f32[32,1024]{1,0:T(8,128)S(1)} %multiply_add_fusion) | copy-start | bytes 393220
  142.5 11.5 %copy-start.5 = (bf16[32,2048]{1,0:T(8,128)(2,1)S(1)}, bf16[32,2048]{1,0:T(8,128)(2,1)}, u32[]{:S(2)}) copy-start(bf16[32,2048]{1,0:T(8,128)(2,1)} %reduce-scatter.3.cloned.1.call-done) | copy-start | bytes 393220
  154.0 48.5 %copy-start.1 = (bf16[32,4096]{1,0:T(8,128)(2,1)S(1)}, bf16[32,4096]{1,0:T(8,128)(2,1)}, u32[]{:S(2)}) copy-start(bf16[32,4096]{1,0:T(8,128)(2,1)} %param.21) | copy-start | bytes 786436
  154.0 49.6 %copy-start.8 = (f32[4096]{0:T(1024)S(1)}, f32[4096]{0:T(1024)}, u32[]{:S(2)}) copy-start(f32[4096]{0:T(1024)} %param.32) | copy-start | bytes 49156
  154.0 64.9 %copy-start.13 = (bf16[512,512]{1,0:T(8,128)(2,1)S(1)}, bf16[512,512]{1,0:T(8,128)(2,1)}, u32[]{:S(2)}) copy-start(bf16[512,512]{1,0:T(8,128)(2,1)} %param.39) | copy-start | bytes 1572868
  154.0 64.9 %copy-start.14 = (bf16[512,512]{1,0:T(8,128)(2,1)S(1)}, bf16[512,512]{1,0:T(8,128)(2,1)}, u32[]{:S(2)}) copy-start(bf16[512,512]{1,0:T(8,128)(2,1)} %param.38) | copy-start | bytes 1572868
  160.7 60.0 %copy-start.10 = (s32[32,2]{0,1:T(2,128)S(1)}, s32[32,2]{0,1:T(2,128)}, u32[]{:S(2)}) copy-start(s32[32,2]{0,1:T(2,128)} %param.34) | copy-start | bytes 772
  160.8 90.2 %reduce-scatter.5.cloned.1.call-start = ((), (), s32[]{:S(2)}) async-start(), calls=%async_computation.8 | async-start | bytes 589824 | tf_op jit(solution)/shard_map/reduce_scatter | solution.py:137
  220.1 81.4 %all-gather.4.cloned.1.call-start = ((), (), s32[]{:S(2)}) async-start(), calls=%async_computation.9 | async-start | bytes 4718592 | tf_op jit(solution)/shard_map/all_gather | solution.py:150
  222.9 82.4 %all-to-all-start.1 = ((bf16[8,16,4096]{2,1,0:T(8,128)(2,1)}), bf16[8,16,4096]{2,1,0:T(8,128)(2,1)S(1)}, u32[]{:S(2)}, u32[]{:S(2)}) async-start(bf16[8,16,4096]{2,1,0:T(8,128)(2,1)} %bitcast.12), calls=%async_computation.2 | async-start | bytes 2097152 | tf_op jit(solution)/shard_map/all_to_all | solution.py:119
  226.5 143.0 %all-reduce.6.cloned.1.call-start = ((), (), s32[]{:S(2)}) async-start(), calls=%async_computation.11 | async-start | bytes 2621440 | tf_op jit(solution)/shard_map/psum | solution.py:126
  308.2 65.9 %copy-start.11 = (bf16[4096]{0:T(1024)(128)(2,1)S(1)}, bf16[4096]{0:T(1024)(128)(2,1)}, u32[]{:S(2)}) copy-start(bf16[4096]{0:T(1024)(128)(2,1)} %param.41) | copy-start | bytes 24580
  308.2 66.6 %copy-start.7 = (bf16[4096,8]{0,1:T(8,128)(2,1)S(1)}, bf16[4096,8]{0,1:T(8,128)(2,1)}, u32[]{:S(2)}) copy-start(bf16[4096,8]{0,1:T(8,128)(2,1)} %param.33) | copy-start | bytes 196612
  314.1 86.5 %copy-start.2 = (bf16[32,4096]{1,0:T(8,128)(2,1)S(1)}, bf16[32,4096]{1,0:T(8,128)(2,1)}, u32[]{:S(2)}) copy-start(bf16[32,4096]{1,0:T(8,128)(2,1)} %all-reduce.4.cloned.1.call-done) | copy-start | bytes 786436
  369.5 31.2 %all-to-all-start.2 = ((bf16[8,16,4096]{2,1,0:T(8,128)(2,1)}), bf16[8,16,4096]{2,1,0:T(8,128)(2,1)S(1)}, u32[]{:S(2)}, u32[]{:S(2)}) async-start(bf16[8,16,4096]{2,1,0:T(8,128)(2,1)} %get-tuple-element.3), calls=%async_computation.3 | async-start | bytes 2097152 | tf_op jit(solution)/shard_map/all_to_all | solution.py:127
Sparse Core Ops, SparseCore 0:
  29.0 31.6 reduce-scatter.2
  62.3 80.1 all-gather.5
  160.9 41.5 all-reduce.3
  220.3 30.6 reduce-scatter.4
  252.4 49.1 all-gather.3
  314.3 55.1 all-reduce.5
